TPU v7x, 32 devices: a whole 2x2x4 slice. The times are simulated.
32 devices in a mesh: sp: 8 (over z, x), tp: 4 (over y, core).
Axes of the slice: x: 2, y: 2, z: 4, core: 2. Of those that a mesh axis runs over, the one named last changes fastest.
Arguments:
- tokens: bfloat16 [4096, 2048], P(('sp', 'tp')), may hold values from -64 to 64
- query_weight: bfloat16 [2048, 2048], P(None, 'tp'), may hold values from -0.125 to 0.125
- key_weight: bfloat16 [2048, 2048], P(None, 'tp'), may hold values from -0.125 to 0.125
- value_weight: bfloat16 [2048, 2048], P(None, 'tp'), may hold values from -0.125 to 0.125
- gate_weight: bfloat16 [2048, 2048], P(None, 'tp'), may hold values from -0.125 to 0.125
- forget_weight: bfloat16 [2048, 16], replicated, may hold values from -0.125 to 0.125
- forget_bias: float32 [16], replicated, as said below
- out_weight: bfloat16 [2048, 2048], replicated, may hold values from -0.125 to 0.125
Outputs:
- mixed: bfloat16 [4096, 2048], P(('sp', 'tp'))
Inputs may be any that keep to these rules, and one draw needn't show every extreme that they name: `forget_bias`: every head's forget bias is at least 4.
All inputs are finite; a program needn't handle non-finite values.
Results may differ from a plain program's by a relative error of at most 0.015.
The roundings to bfloat16 on the way count: a program that leaves them out, or rounds other values in their place, can miss the bound.
Values may be sent and summed in bfloat16 or wider, within the bound.
A program may use at most 128 MiB of HBM per device.

v0:
```python
import math

import jax
import jax.numpy as jnp
from jax import lax
from jax.sharding import PartitionSpec as P

HEAD_DIM = 128


def body(
    tokens,
    query_weight,
    key_weight,
    value_weight,
    gate_weight,
    forget_weight,
    forget_bias,
    out_weight,
):
    width = query_weight.shape[1]
    heads_dev = width // HEAD_DIM
    first_head = lax.axis_index("tp") * heads_dev
    piece = lax.all_gather(tokens, "tp", axis=0, tiled=True)
    products = [
        jnp.dot(piece, weight, preferred_element_type=jnp.float32)
        for weight in (query_weight, key_weight, value_weight, gate_weight, forget_weight)
    ]
    joined = jnp.concatenate(products, axis=1)
    rows = joined.shape[0]
    queries = (
        (joined[:, :width] * HEAD_DIM ** (-0.5))
        .astype(jnp.bfloat16)
        .reshape(rows, heads_dev, HEAD_DIM)
    )
    keys = joined[:, width : 2 * width].astype(jnp.bfloat16)
    values = joined[:, 2 * width : 3 * width].astype(jnp.bfloat16)
    gate = jax.nn.sigmoid(joined[:, 3 * width : 4 * width])
    logits = lax.dynamic_slice_in_dim(joined[:, 4 * width :], first_head, heads_dev, 1)
    bias = lax.dynamic_slice_in_dim(forget_bias, first_head, heads_dev, 0)
    forget_log = jax.nn.log_sigmoid(logits + bias).T
    all_logs = lax.all_gather(forget_log, "sp", axis=1, tiled=True)
    cumul = jnp.cumsum(all_logs, axis=1)
    my_start = lax.axis_index("sp") * rows
    last_query = my_start + rows - 1
    cum_query = lax.dynamic_slice_in_dim(cumul, my_start, rows, 1)
    query_pos = my_start + jnp.arange(rows, dtype=jnp.int32)
    paired = jnp.stack([keys, values])

    def absorb(carry, key_blk, value_blk, key_start):
        best, total, accum = carry
        span = key_blk.shape[0]
        scores = jnp.einsum(
            "qhd,khd->hqk",
            queries,
            key_blk.reshape(span, heads_dev, HEAD_DIM),
            preferred_element_type=jnp.float32,
        )
        cum_key = lax.dynamic_slice_in_dim(cumul, jnp.maximum(key_start, 0), span, 1)
        scores = scores + cum_query[:, :, None] - cum_key[:, None, :]
        key_pos = key_start + jnp.arange(span, dtype=jnp.int32)
        valid = (key_pos[None, :] <= query_pos[:, None]) & (key_pos[None, :] >= 0)
        scores = jnp.where(valid[None], scores, -jnp.inf)
        new_best = jnp.maximum(best, jnp.max(scores, axis=-1))
        factor = jnp.exp(best - new_best)
        weights = jnp.exp(scores - new_best[..., None])
        total = total * factor + jnp.sum(weights, axis=-1)
        accum = accum * factor[..., None] + jnp.einsum(
            "hqk,khd->hqd",
            weights.astype(jnp.bfloat16),
            value_blk.reshape(span, heads_dev, HEAD_DIM),
            preferred_element_type=jnp.float32,
        )
        return (new_best, total, accum)

    initial = (
        jnp.full((heads_dev, rows), -1e30, jnp.float32),
        jnp.zeros((heads_dev, rows), jnp.float32),
        jnp.zeros((heads_dev, rows, HEAD_DIM), jnp.float32),
    )
    carry = initial
    piece = lax.all_gather(paired, "sp", axis=1, tiled=True)
    length = piece.shape[1]
    span = math.gcd(length, 512)
    steps = length // span
    key_blocks = piece[0].reshape(steps, span, width)
    value_blocks = piece[1].reshape(steps, span, width)
    offsets = jnp.arange(steps, dtype=jnp.int32) * span

    def one(state, inputs):
        state = lax.cond(
            inputs[2] <= last_query,
            lambda inner: absorb(inner, inputs[0], inputs[1], inputs[2]),
            lambda inner: inner,
            state,
        )
        return (state, None)

    carry, _ = lax.scan(one, carry, (key_blocks, value_blocks, offsets))
    best, total, accum = carry
    heads_out = (accum / total[..., None]).transpose(1, 0, 2).reshape(rows, width)
    attended = (heads_out * gate).astype(jnp.bfloat16)
    regrouped = lax.all_to_all(attended, "tp", split_axis=0, concat_axis=1, tiled=True)
    mixed = jnp.dot(regrouped, out_weight, preferred_element_type=jnp.float32)
    return mixed.astype(jnp.bfloat16)


def solution(mesh):
    placed = (
        P(("sp", "tp"), None),
        P(None, "tp"),
        P(None, "tp"),
        P(None, "tp"),
        P(None, "tp"),
        P(),
        P(),
        P(),
    )
    return jax.shard_map(
        body, mesh=mesh, in_specs=placed, out_specs=P(("sp", "tp"), None), check_vma=False
    )
```

profile of v0, /device:TPU:26, one launch (start us, length us, event | category | flops | bytes accessed | tf_op | source)
XLA Modules:
  0.0 293.6 jit_solution(11329461821826093112)
XLA Ops:
  6.5 0.7 all-gather.3.cloned.1.call-update
  7.3 25.1 %all-gather.3.cloned.1.call-done = bf16[512,2048]{1,0:T(8,128)(2,1)} async-done(((bf16[128,2048]{1,0:T(8,128)(2,1)}), bf16[512,2048]{1,0:T(8,128)(2,1)}) %all-gather.3.cloned.1.call-update) | async-done | bytes 2097168 | tf_op jit(solution)/shard_map/all_gather | solution.py:24
  32.5 3.0 %fusion.18 = bf16[1,512,512]{2,1,0:T(8,128)(2,1)S(1)} fusion(bf16[512,2048]{1,0:T(8,128)(2,1)} %all-gather.3.cloned.1.call-done, bf16[2048,512]{1,0:T(8,128)(2,1)S(1)} %copy-done), kind=kOutput, calls=%fused_computation.30 | convolution fusion | flops 1074003968 | bytes 4718592 | tf_op jit(solution)/shard_map/dot_general | solution.py:26
  35.5 1.2 fusion.19
  36.7 1.1 pad_maximum_fusion
  38.0 2.2 fusion.23
  40.3 31.8 %all_gather.11 = f32[4,4096]{1,0:T(4,128)S(1)} all-gather(f32[4,512]{1,0:T(4,128)S(1)} %fusion.21), channel_id=1, replica_groups=mesh['sp'=8,'tp'=4] {'sp'}, dimensions={1}, use_global_device_ids=true | all-gather | bytes 73728 | tf_op jit(solution)/shard_map/all_gather | solution.py:42
  72.1 1.2 reduce-window.6
  73.8 3.5 %fusion.17 = bf16[512,512]{0,1:T(8,128)(2,1)S(1)} fusion(bf16[512,2048]{1,0:T(8,128)(2,1)} %all-gather.3.cloned.1.call-done, bf16[2048,512]{1,0:T(8,128)(2,1)} %param.13), kind=kOutput, calls=%fused_computation.29 | convolution fusion | flops 1074266112 | bytes 4718592 | tf_op jit(solution)/shard_map/dot_general | solution.py:26
  77.3 1.0 copy.16
  78.3 81.7 %all-gather.5.cloned.1.call-done = bf16[2,4096,512]{2,1,0:T(8,128)(2,1)} async-done(((bf16[2,512,512]{2,1,0:T(8,128)(2,1)}), bf16[2,4096,512]{2,1,0:T(8,128)(2,1)}) %all-gather.5.cloned.1.call-update) | async-done | bytes 8388624 | tf_op jit(solution)/shard_map/all_gather | solution.py:82
  160.0 5.7 %fusion.22 = (bf16[1,4096,512]{2,1,0:T(8,128)(2,1)}, bf16[1,4096,512]{2,1,0:T(8,128)(2,1)}) fusion(bf16[2,4096,512]{2,1,0:T(8,128)(2,1)} %all-gather.5.cloned.1.call-done), kind=kLoop, calls=%fused_computation.43 | loop fusion | bytes 16777216 | tf_op jit(solution)/shard_map/slice | solution.py:87
  165.7 6.5 %copy.15 = bf16[8,512,512]{1,2,0:T(8,128)(2,1)} copy(bf16[8,512,512]{2,1,0:T(8,128)(2,1)} %bitcast.61) | data formatting | bytes 8388608
  172.2 6.5 %copy.17 = bf16[8,512,512]{1,2,0:T(8,128)(2,1)} copy(bf16[8,512,512]{2,1,0:T(8,128)(2,1)} %bitcast.60) | data formatting | bytes 8388608
  178.8 85.4 %while.15 = (s32[]{:T(128)}, f32[4,512]{1,0:T(4,128)S(1)}, f32[4,512]{1,0:T(4,128)S(1)}, f32[4,512,128]{2,1,0:T(8,128)S(1)}, s32[8]{0:T(128)S(1)}, /*index=5*/s3...) while((s32[]{:T(128)}, f32[4,512]{1,0:T(4,128)S(1)}, ...), condition=%wide.region_7.8_spmd.clone, body=%wide.region_2.7_spmd.clone.sunk | while | flops 552605696 | bytes 19608912 | solution.py:99
  180.1 9.4 %conditional.3 = ((f32[4,512]{1,0:T(4,128)S(1)}, f32[4,512]{1,0:T(4,128)S(1)}, f32[4,512,128]{2,1,0:T(8,128)S(1)})) conditional(s32[]{:T(128)} %convert_element_type.43, (f32[4,512]{1,0:T(4,128)S(1)}, f32[4,512]{1,0:T(4,128)S(1)}, f32[4,512,128]{2,1,0:T(8,128)S(1)}) %tuple.43, (s32[]{:T(128)}, s32[]{:T(128)}, bf16[8,512,512]{1,2,0:T(8,128)(2,1)}, ...), branch_computations={%region_3.3_spmd, %region_4.6_spmd} | conditional | flops 552605696 | bytes 19606592 | solution.py:91
  182.3 1.3 constant_dynamic-slice_fusion
  183.6 2.3 fusion.4
  185.9 1.2 fusion.3
  187.2 2.2 fusion.8
  189.5 0.6 dynamic_slice.45
  190.7 9.4 %conditional.3 = ((f32[4,512]{1,0:T(4,128)S(1)}, f32[4,512]{1,0:T(4,128)S(1)}, f32[4,512,128]{2,1,0:T(8,128)S(1)})) conditional(s32[]{:T(128)} %convert_element_type.43, (f32[4,512]{1,0:T(4,128)S(1)}, f32[4,512]{1,0:T(4,128)S(1)}, f32[4,512,128]{2,1,0:T(8,128)S(1)}) %tuple.43, (s32[]{:T(128)}, s32[]{:T(128)}, bf16[8,512,512]{1,2,0:T(8,128)(2,1)}, ...), branch_computations={%region_3.3_spmd, %region_4.6_spmd} | conditional | flops 552605696 | bytes 19606592 | solution.py:91
  193.0 1.3 constant_dynamic-slice_fusion
  194.2 2.3 fusion.4
  196.6 1.2 fusion.3
  197.9 2.2 fusion.8
  200.1 0.6 dynamic_slice.45
  201.4 9.4 %conditional.3 = ((f32[4,512]{1,0:T(4,128)S(1)}, f32[4,512]{1,0:T(4,128)S(1)}, f32[4,512,128]{2,1,0:T(8,128)S(1)})) conditional(s32[]{:T(128)} %convert_element_type.43, (f32[4,512]{1,0:T(4,128)S(1)}, f32[4,512]{1,0:T(4,128)S(1)}, f32[4,512,128]{2,1,0:T(8,128)S(1)}) %tuple.43, (s32[]{:T(128)}, s32[]{:T(128)}, bf16[8,512,512]{1,2,0:T(8,128)(2,1)}, ...), branch_computations={%region_3.3_spmd, %region_4.6_spmd} | conditional | flops 552605696 | bytes 19606592 | solution.py:91
  203.6 1.3 constant_dynamic-slice_fusion
  204.9 2.3 fusion.4
  207.3 1.2 fusion.3
  208.5 2.2 fusion.8
  212.1 9.4 %conditional.3 = ((f32[4,512]{1,0:T(4,128)S(1)}, f32[4,512]{1,0:T(4,128)S(1)}, f32[4,512,128]{2,1,0:T(8,128)S(1)})) conditional(s32[]{:T(128)} %convert_element_type.43, (f32[4,512]{1,0:T(4,128)S(1)}, f32[4,512]{1,0:T(4,128)S(1)}, f32[4,512,128]{2,1,0:T(8,128)S(1)}) %tuple.43, (s32[]{:T(128)}, s32[]{:T(128)}, bf16[8,512,512]{1,2,0:T(8,128)(2,1)}, ...), branch_computations={%region_3.3_spmd, %region_4.6_spmd} | conditional | flops 552605696 | bytes 19606592 | solution.py:91
  214.3 1.3 constant_dynamic-slice_fusion
  215.6 2.3 fusion.4
  217.9 1.2 fusion.3
  219.2 2.2 fusion.8
  221.5 0.6 dynamic_slice.45
  222.7 9.4 %conditional.3 = ((f32[4,512]{1,0:T(4,128)S(1)}, f32[4,512]{1,0:T(4,128)S(1)}, f32[4,512,128]{2,1,0:T(8,128)S(1)})) conditional(s32[]{:T(128)} %convert_element_type.43, (f32[4,512]{1,0:T(4,128)S(1)}, f32[4,512]{1,0:T(4,128)S(1)}, f32[4,512,128]{2,1,0:T(8,128)S(1)}) %tuple.43, (s32[]{:T(128)}, s32[]{:T(128)}, bf16[8,512,512]{1,2,0:T(8,128)(2,1)}, ...), branch_computations={%region_3.3_spmd, %region_4.6_spmd} | conditional | flops 552605696 | bytes 19606592 | solution.py:91
  225.0 1.3 constant_dynamic-slice_fusion
  226.2 2.3 fusion.4
  228.6 1.2 fusion.3
  229.9 2.2 fusion.8
  232.1 0.6 dynamic_slice.45
  233.4 9.4 %conditional.3 = ((f32[4,512]{1,0:T(4,128)S(1)}, f32[4,512]{1,0:T(4,128)S(1)}, f32[4,512,128]{2,1,0:T(8,128)S(1)})) conditional(s32[]{:T(128)} %convert_element_type.43, (f32[4,512]{1,0:T(4,128)S(1)}, f32[4,512]{1,0:T(4,128)S(1)}, f32[4,512,128]{2,1,0:T(8,128)S(1)}) %tuple.43, (s32[]{:T(128)}, s32[]{:T(128)}, bf16[8,512,512]{1,2,0:T(8,128)(2,1)}, ...), branch_computations={%region_3.3_spmd, %region_4.6_spmd} | conditional | flops 552605696 | bytes 19606592 | solution.py:91
  235.6 1.3 constant_dynamic-slice_fusion
  236.9 2.3 fusion.4
  239.3 1.2 fusion.3
  240.5 2.2 fusion.8
  242.8 0.6 dynamic_slice.45
  244.1 9.4 %conditional.3 = ((f32[4,512]{1,0:T(4,128)S(1)}, f32[4,512]{1,0:T(4,128)S(1)}, f32[4,512,128]{2,1,0:T(8,128)S(1)})) conditional(s32[]{:T(128)} %convert_element_type.43, (f32[4,512]{1,0:T(4,128)S(1)}, f32[4,512]{1,0:T(4,128)S(1)}, f32[4,512,128]{2,1,0:T(8,128)S(1)}) %tuple.43, (s32[]{:T(128)}, s32[]{:T(128)}, bf16[8,512,512]{1,2,0:T(8,128)(2,1)}, ...), branch_computations={%region_3.3_spmd, %region_4.6_spmd} | conditional | flops 552605696 | bytes 19606592 | solution.py:91
  246.3 1.3 constant_dynamic-slice_fusion
  247.6 2.3 fusion.4
  249.9 1.2 fusion.3
  251.2 2.2 fusion.8
  254.8 9.4 %conditional.3 = ((f32[4,512]{1,0:T(4,128)S(1)}, f32[4,512]{1,0:T(4,128)S(1)}, f32[4,512,128]{2,1,0:T(8,128)S(1)})) conditional(s32[]{:T(128)} %convert_element_type.43, (f32[4,512]{1,0:T(4,128)S(1)}, f32[4,512]{1,0:T(4,128)S(1)}, f32[4,512,128]{2,1,0:T(8,128)S(1)}) %tuple.43, (s32[]{:T(128)}, s32[]{:T(128)}, bf16[8,512,512]{1,2,0:T(8,128)(2,1)}, ...), branch_computations={%region_3.3_spmd, %region_4.6_spmd} | conditional | flops 552605696 | bytes 19606592 | solution.py:91
  257.0 1.3 constant_dynamic-slice_fusion
  258.3 2.3 fusion.4
  260.6 1.2 fusion.3
  261.9 2.2 fusion.8
  264.1 4.5 %fusion.16 = bf16[512,512]{1,0:T(8,128)(2,1)} fusion(bf16[512,2048]{1,0:T(8,128)(2,1)} %all-gather.3.cloned.1.call-done, bf16[2048,512]{1,0:T(8,128)(2,1)} %param.16, f32[4,512,128]{2,1,0:T(8,128)S(1)} %get-tuple-element.165, f32[4,512]{1,0:T(4,128)S(1)} %get-tuple-element.166), kind=kOutput, calls=%fused_computation.26 | convolution fusion | flops 1075314688 | bytes 5775360 | tf_op jit(solution)/shard_map/dot_general | solution.py:26
  268.6 1.3 copy.19
  269.9 11.4 %all_to_all.19 = bf16[4,128,512]{1,2,0:T(8,128)(2,1)S(1)} all-to-all(bf16[4,128,512]{1,2,0:T(8,128)(2,1)S(1)} %copy.19), channel_id=1, replica_groups=mesh['sp'=8,'tp'=4] {'tp'}, dimensions={0} | all-to-all | bytes 1048576 | tf_op jit(solution)/shard_map/all_to_all | solution.py:103
  281.3 5.5 %convolution_convert_fusion = bf16[128,2048]{1,0:T(8,128)(2,1)} fusion(bf16[128,2048]{0,1:T(8,128)(2,1)S(1)} %bitcast.64, bf16[2048,2048]{1,0:T(8,128)(2,1)} %param.19), kind=kOutput, calls=%fused_computation.19 | convolution fusion | flops 1074003968 | bytes 9437184 | tf_op jit(solution)/shard_map/dot_general | solution.py:104
  (92 shorter events, 15.6 us)
Async XLA Ops:
  6.5 25.9 %copy-start = (bf16[2048,512]{1,0:T(8,128)(2,1)S(1)}, bf16[2048,512]{1,0:T(8,128)(2,1)}, u32[]{:S(2)}) copy-start(bf16[2048,512]{1,0:T(8,128)(2,1)} %param.14) | copy-start | bytes 6291460
  6.5 25.9 %all-gather.3.cloned.1.call-start = ((), (), s32[]{:S(2)}) async-start(), calls=%async_computation.1 | async-start | bytes 2621440 | tf_op jit(solution)/shard_map/all_gather | solution.py:24
  7.3 152.7 %all-gather.5.cloned.1.call-start = ((), (), s32[]{:S(2)}) async-start(), calls=%async_computation.2 | async-start | bytes 9437184 | tf_op jit(solution)/shard_map/all_gather | solution.py:82
  32.4 3.0 %copy-start.1 = (bf16[512,2048]{1,0:T(8,128)(2,1)S(1)}, bf16[512,2048]{1,0:T(8,128)(2,1)}, u32[]{:S(2)}) copy-start(bf16[512,2048]{1,0:T(8,128)(2,1)} %all-gather.3.cloned.1.call-done) | copy-start | bytes 6291460
  32.4 3.0 %copy-start.3 = (bf16[2048,512]{1,0:T(8,128)(2,1)S(1)}, bf16[2048,512]{1,0:T(8,128)(2,1)}, u32[]{:S(2)}) copy-start(bf16[2048,512]{1,0:T(8,128)(2,1)} %param.15) | copy-start | bytes 6291460
  35.5 2.4 copy-start.4
  35.5 2.5 copy-start.2
Sparse Core Ops, SparseCore 0:
  8.9 23.5 all-gather.2
  38.0 121.9 all-gather.4
where the time goes:
time: 295 us; the launch traced here: 294 us
  waiting for transfers between devices  108 us (37%)
  matrix products  56.4 us (19%)
  blocking collectives  43.1 us (15%)
  local copies, waits for them, and re-layouts  37.4 us (13%)
  other arithmetic  24.8 us (8%)
  between operations  13.5 us (5%)
  loops' own time  10.8 us (4%)
    all_gather x1, waiting for transfers between devices, body(): piece = lax.all_gather(paired, 'sp', axis=1, tiled=True)  81.7 us
    all_gather x1, blocking collectives, body(): all_logs = lax.all_gather(forget_log, 'sp', axis=1, tiled=True)  31.8 us
    all_gather x1, waiting for transfers between devices, body(): piece = lax.all_gather(tokens, 'tp', axis=0, tiled=True)  25.1 us
    dot_general x8, matrix products, absorb(): jnp.einsum('qhd,khd->hqk', queries, key_blk.reshape(span, heads_dev, HEAD...  18.7 us
    dot_general x8, matrix products, absorb(): jnp.einsum('hqk,khd->hqd', weights.astype(jnp.bfloat16), value_blk.reshap...  17.8 us
    dynamic_slice x16, local copies, waits for them, and re-layouts, body(): carry, _ = lax.scan(one, carry, (key_blocks, value_blocks, offsets))  15.3 us
    dot_general x5, matrix products, body(): jnp.dot(piece, weight, preferred_element_type=jnp.float32)  14.4 us
    unnamed x15, local copies, waits for them, and re-layouts  14.1 us
  transfers between devices with their start and end apart: 2, of which 2 were waited for; matrix products, arithmetic and copies ran while one was open for 3% of the time, Pallas kernels for 0%

commit v1 on v0

v1 whole, which is shorter than its diff:
```python
import functools

import jax
import jax.numpy as jnp
from jax import lax
from jax.experimental import pallas as pl
from jax.experimental.pallas import tpu as pltpu
from jax.sharding import PartitionSpec as P

HEAD_DIM = 128
CORES = 2
MESH = pl.DeviceIdType.MESH
F32 = jnp.float32
BF16 = jnp.bfloat16


def kernel(
    dims,
    x_hbm, wq_hbm, wk_hbm, wv_hbm, wg_hbm, fw_ref, fb_ref, wo_hbm,
    out_ref,
    tok, wbuf, wo, kvs, qs_, gs, fs, kvd, qd, fd, crow, obuf, oin, gin, att,
    m_ref, l_ref, acc_ref,
    load_sem, tok_send, tok_recv, tok_fwd,
    kv_send, f_send, q_send, g_send, kv_fwd, f_fwd,
    kv_recv, f_recv, q_recv, g_recv, o_send, o_recv,
):
    S, T, td, D, hd = dims
    H = T * hd
    rows = T * td
    ny = T // CORES
    gr = CORES * td
    hp = CORES * hd
    cph = S // hp
    G = CORES * cph
    seq = S * rows
    ng = S * ny
    ch = seq // (2 * G)
    qt = min(512, ch)
    kb = qt
    width = hd * HEAD_DIM
    s = lax.axis_index("sp")
    t = lax.axis_index("tp")
    y = t // CORES
    c = t % CORES
    peer = y * CORES + (1 - c)

    def remote(src, dst, ssem, rsem, ds, dt):
        return pltpu.make_async_remote_copy(
            src_ref=src, dst_ref=dst, send_sem=ssem, recv_sem=rsem,
            device_id={"sp": ds, "tp": dt}, device_id_type=MESH,
        )

    def send(src, dst, ssem, rsem, ds, dt):
        mine = jnp.logical_and(ds == s, dt == t)

        @pl.when(mine)
        def _():
            pltpu.make_async_copy(src, dst, rsem).start()

        @pl.when(jnp.logical_not(mine))
        def _():
            remote(src, dst, ssem, rsem, ds, dt).start()

    def sent(src, dst, ssem, rsem, ds, dt):
        mine = jnp.logical_and(ds == s, dt == t)

        @pl.when(jnp.logical_not(mine))
        def _():
            remote(src, dst, ssem, rsem, ds, dt).wait_send()

    def arrived(dst, rsem):
        pltpu.make_async_copy(dst, dst, rsem).wait()

    def piece(i):
        return tok.at[pl.ds(pl.multiple_of(i * td, td), td)]

    own = pltpu.make_async_copy(x_hbm, piece(t), load_sem.at[0])
    own.start()
    loads = []
    for i, w in enumerate((wk_hbm, wv_hbm, wq_hbm, wg_hbm)):
        loads.append(pltpu.make_async_copy(w, wbuf.at[i], load_sem.at[1 + i]))
    loads.append(pltpu.make_async_copy(wo_hbm, wo, load_sem.at[5]))
    for ld in loads:
        ld.start()
    own.wait()
    tok_copies = []
    for dy in range(1, ny):
        dt = ((y + dy) % ny) * CORES + c
        tok_copies.append(remote(piece(t), piece(t), tok_send.at[dy], tok_recv.at[t], s, dt))
    tok_copies.append(remote(piece(t), piece(t), tok_send.at[0], tok_recv.at[t], s, peer))
    for cp in tok_copies:
        cp.start()
    arrived(piece(peer), tok_recv.at[peer])

    lane = lax.broadcasted_iota(jnp.int32, (H, gr), 1)

    def q_place(b):
        start = b * gr
        ci = start // ch
        late = ci // G
        r = ci + late * (2 * G - 1 - 2 * ci)
        return r, pl.multiple_of(late * ch + start % ch, gr)

    def kv_args(dy, yg, j, m):
        b = s * ny + yg
        jj = c * hd + j
        at = (dy * hd + j) * cph + m
        dst_s = jj * cph + m
        dst_t = y * CORES + s % CORES
        base = pl.multiple_of(yg * gr, gr)
        gbase = pl.multiple_of(b * gr, gr)
        return (
            (kvs.at[j, pl.ds(base, gr)], kvd.at[pl.ds(gbase, gr)], kv_send.at[at], kv_recv.at[b], dst_s, dst_t),
            (fs.at[dy, t * hd + j], fd.at[b], f_send.at[at], f_recv.at[b], dst_s, dst_t),
        )

    def q_args(dy, yg, j):
        b = s * ny + yg
        jj = c * hd + j
        r, pos = q_place(b)
        base = pl.multiple_of(yg * gr, gr)
        return (
            qs_.at[j, pl.ds(base, gr)], qd.at[pl.ds(pos, gr)], q_send.at[dy * hd + j],
            q_recv.at[pos // gr], jj * cph + r // CORES, y * CORES + r % CORES,
        )

    def g_args(dt):
        return (
            gs.at[:, pl.ds(pl.multiple_of(dt * td, td), td)], gin.at[pl.ds(t * hd, hd)],
            g_send.at[dt], g_recv.at[t], s, dt,
        )

    for dy in range(ny):
        yg = (y + dy) % ny
        base = pl.multiple_of(yg * gr, gr)
        if dy > 0:
            got = yg * CORES + c
            other = yg * CORES + 1 - c
            arrived(piece(got), tok_recv.at[got])
            remote(piece(got), piece(got), tok_fwd.at[dy], tok_recv.at[got], s, peer).start()
            arrived(piece(other), tok_recv.at[other])
        x = tok[pl.ds(base, gr), :]
        if dy == 0:
            loads[0].wait()
        prod = jnp.dot(x, wbuf[0], preferred_element_type=F32)
        for j in range(hd):
            kvs[j, pl.ds(base, gr), 0:HEAD_DIM] = prod[:, j * HEAD_DIM : (j + 1) * HEAD_DIM].astype(BF16)
        if dy == 0:
            loads[1].wait()
        prod = jnp.dot(x, wbuf[1], preferred_element_type=F32)
        for j in range(hd):
            kvs[j, pl.ds(base, gr), HEAD_DIM:] = prod[:, j * HEAD_DIM : (j + 1) * HEAD_DIM].astype(BF16)
        logit = lax.dot_general(
            fw_ref[...], x, (((1,), (1,)), ((), ())), preferred_element_type=F32
        ) + fb_ref[:, 0:1]
        logs = jnp.minimum(logit, 0.0) - jnp.log1p(jnp.exp(-jnp.abs(logit)))
        step = 1
        while step < gr:
            logs = logs + jnp.where(lane >= step, pltpu.roll(logs, step, 1), 0.0)
            step *= 2
        for h in range(H):
            fs[dy, h] = jnp.broadcast_to(logs[h : h + 1, :], (8, gr))
        for j in range(hd):
            for m in range(cph):
                kv, f = kv_args(dy, yg, j, m)
                send(*kv)
                send(*f)
        if dy == 0:
            loads[2].wait()
        prod = jnp.dot(x, wbuf[2], preferred_element_type=F32) * HEAD_DIM ** (-0.5)
        for j in range(hd):
            qs_[j, pl.ds(base, gr)] = prod[:, j * HEAD_DIM : (j + 1) * HEAD_DIM].astype(BF16)
        for j in range(hd):
            send(*q_args(dy, yg, j))
        if dy == 0:
            loads[3].wait()
        prod = jax.nn.sigmoid(jnp.dot(x, wbuf[3], preferred_element_type=F32))
        for j in range(hd):
            gs[j, pl.ds(base, gr)] = prod[:, j * HEAD_DIM : (j + 1) * HEAD_DIM]
        for e in range(CORES):
            send(*g_args(yg * CORES + e))

    def fwd_args(b):
        gbase = pl.multiple_of(b * gr, gr)
        at = (b // ny) // CORES * ny + b % ny
        blk = kvd.at[pl.ds(gbase, gr)]
        return (
            (blk, blk, kv_fwd.at[at], kv_recv.at[b], s, peer),
            (fd.at[b], fd.at[b], f_fwd.at[at], f_recv.at[b], s, peer),
        )

    def fwd_block(i, parity):
        return ((i // ny) * CORES + parity) * ny + i % ny

    def forward(i, carry):
        b = fwd_block(i, c)
        kv, f = fwd_args(b)
        arrived(f[0], f_recv.at[b])
        remote(*f).start()
        arrived(kv[0], kv_recv.at[b])
        remote(*kv).start()
        return carry

    lax.fori_loop(0, ng // CORES, forward, 0)

    def collect(i, carry):
        b = fwd_block(i, 1 - c)
        kv, f = fwd_args(b)
        arrived(f[0], f_recv.at[b])
        arrived(kv[0], kv_recv.at[b])
        return carry

    lax.fori_loop(0, ng // CORES, collect, 0)

    def q_wait(i, carry):
        arrived(qd.at[pl.ds(pl.multiple_of(i * gr, gr), gr)], q_recv.at[i])
        return carry

    lax.fori_loop(0, 2 * ch // gr, q_wait, 0)

    def chain(b, offset):
        blk = fd[b] + offset
        crow[:, pl.ds(pl.multiple_of(b * gr, gr), gr)] = blk
        return blk[:, gr - 1 : gr]

    lax.fori_loop(0, ng, chain, jnp.zeros((8, 1), F32))

    r = (s % cph) * CORES + c
    head = y * hp + s // cph
    above = lax.broadcasted_iota(jnp.int32, (qt, kb), 1) > lax.broadcasted_iota(jnp.int32, (qt, kb), 0)

    def o_args(half, u):
        ci = r if half == 0 else 2 * G - 1 - r
        token = ci * ch + u * td
        at = half * (ch // td) + u
        return (
            obuf.at[pl.ds(pl.multiple_of(half * ch + u * td, td), td)], oin.at[head],
            o_send.at[at], o_recv.at[head], token // rows, (token % rows) // td,
        )

    for half in range(2):
        ci = r if half == 0 else 2 * G - 1 - r
        for tile in range(ch // qt):
            at = half * ch + tile * qt
            q0 = pl.multiple_of(ci * ch + tile * qt, qt)
            q = qd[at : at + qt, :]
            cq = crow[:, pl.ds(q0, qt)]
            c0 = cq[0:1, 0:1]
            cqc = (cq - c0).T[:, 0:1]
            m_ref[...] = jnp.full(m_ref.shape, -1e30, F32)
            l_ref[...] = jnp.zeros(l_ref.shape, F32)
            acc_ref[...] = jnp.zeros(acc_ref.shape, F32)

            def absorb(kblk, masked, q=q, c0=c0, cqc=cqc):
                k0 = pl.multiple_of(kblk * kb, kb)
                scores = lax.dot_general(
                    q, kvd[pl.ds(k0, kb), 0:HEAD_DIM], (((1,), (1,)), ((), ())),
                    preferred_element_type=F32,
                )
                scores = scores + (c0 - crow[0:1, pl.ds(k0, kb)])
                if masked:
                    scores = jnp.where(above, -jnp.inf, scores)
                best = m_ref[:, 0:1]
                top = jnp.maximum(best, jnp.max(scores, axis=1, keepdims=True) + cqc)
                factor = jnp.exp(best - top)
                weights = jnp.exp(scores - (top - cqc))
                part = weights[:, 0:128]
                for i in range(1, kb // 128):
                    part = part + weights[:, i * 128 : (i + 1) * 128]
                l_ref[...] = l_ref[...] * factor + part
                acc_ref[...] = acc_ref[...] * factor + jnp.dot(
                    weights.astype(BF16), kvd[pl.ds(k0, kb), HEAD_DIM:], preferred_element_type=F32
                )
                m_ref[...] = jnp.broadcast_to(top, m_ref.shape)

            full = q0 // kb

            def full_step(i, carry):
                absorb(i, False)
                return carry

            lax.fori_loop(0, full, full_step, 0)
            absorb(full, True)
            total = jnp.sum(l_ref[...], axis=1, keepdims=True)
            obuf[at : at + qt, :] = (acc_ref[...] / total).astype(BF16)
            for u in range(qt // td):
                send(*o_args(half, tile * (qt // td) + u))

    def g_wait(i, carry):
        arrived(gin.at[pl.ds(i * hd, hd)], g_recv.at[i])
        return carry

    lax.fori_loop(0, T, g_wait, 0)
    loads[4].wait()
    for h in range(H):
        arrived(oin.at[h], o_recv.at[h])
        att[:, h * HEAD_DIM : (h + 1) * HEAD_DIM] = (oin[h].astype(F32) * gin[h]).astype(BF16)
    cols = 512
    for n in range(D // cols):
        out_ref[:, n * cols : (n + 1) * cols] = jnp.dot(
            att[...], wo[:, n * cols : (n + 1) * cols], preferred_element_type=F32
        ).astype(BF16)

    for cp in tok_copies:
        cp.wait_send()
    for dy in range(ny):
        yg = (y + dy) % ny
        if dy > 0:
            got = yg * CORES + c
            remote(piece(got), piece(got), tok_fwd.at[dy], tok_recv.at[got], s, peer).wait_send()
        for j in range(hd):
            for m in range(cph):
                kv, f = kv_args(dy, yg, j, m)
                sent(*kv)
                sent(*f)
            sent(*q_args(dy, yg, j))
        for e in range(CORES):
            sent(*g_args(yg * CORES + e))

    def fwd_done(i, carry):
        kv, f = fwd_args(fwd_block(i, c))
        remote(*f).wait_send()
        remote(*kv).wait_send()
        return carry

    lax.fori_loop(0, ng // CORES, fwd_done, 0)
    for half in range(2):
        for u in range(ch // td):
            sent(*o_args(half, u))


def body(tokens, wq, wk, wv, wg, fw, fb, wo, *, S, T):
    td, D = tokens.shape
    width = wq.shape[1]
    hd = width // HEAD_DIM
    H = T * hd
    rows = T * td
    ny = T // CORES
    gr = CORES * td
    hp = CORES * hd
    cph = S // hp
    G = CORES * cph
    seq = S * rows
    ng = S * ny
    ch = seq // (2 * G)
    qt = min(512, ch)
    dma = pltpu.SemaphoreType.DMA
    vmem = pltpu.VMEM
    any_ = pl.BlockSpec(memory_space=pl.ANY)
    vm = pl.BlockSpec(memory_space=pltpu.VMEM)
    scratch = [
        vmem((rows, D), BF16), vmem((4, D, width), BF16), vmem((D, D), BF16),
        vmem((hd, rows, 2 * HEAD_DIM), BF16), vmem((hd, rows, HEAD_DIM), BF16),
        vmem((hd, rows, HEAD_DIM), F32), vmem((ny, H, 8, gr), F32),
        vmem((seq, 2 * HEAD_DIM), BF16), vmem((2 * ch, HEAD_DIM), BF16),
        vmem((ng, 8, gr), F32), vmem((8, seq), F32), vmem((2 * ch, HEAD_DIM), BF16),
        vmem((H, td, HEAD_DIM), BF16), vmem((H, td, HEAD_DIM), F32), vmem((td, D), BF16),
        vmem((qt, 128), F32), vmem((qt, 128), F32), vmem((qt, HEAD_DIM), F32),
        dma((6,)), dma((ny,)), dma((T,)), dma((ny,)),
        dma((ny * hd * cph,)), dma((ny * hd * cph,)), dma((ny * hd,)), dma((T,)),
        dma((ng // CORES,)), dma((ng // CORES,)),
        dma((ng,)), dma((ng,)), dma((2 * ch // gr,)), dma((T,)), dma((2 * ch // td,)), dma((H,)),
    ]
    return pl.pallas_call(
        functools.partial(kernel, (S, T, td, D, hd)),
        out_shape=jax.ShapeDtypeStruct((td, D), BF16),
        in_specs=[any_, any_, any_, any_, any_, vm, vm, any_],
        out_specs=vm,
        scratch_shapes=scratch,
        compiler_params=pltpu.CompilerParams(
            has_side_effects=True, vmem_limit_bytes=60 * 1024 * 1024
        ),
    )(tokens, wq, wk, wv, wg, fw.T, jnp.broadcast_to(fb[:, None], (H, 128)), wo)


def solution(mesh):
    placed = (
        P(("sp", "tp"), None),
        P(None, "tp"), P(None, "tp"), P(None, "tp"), P(None, "tp"),
        P(), P(), P(),
    )
    run = functools.partial(body, S=mesh.shape["sp"], T=mesh.shape["tp"])
    return jax.shard_map(
        run, mesh=mesh, in_specs=placed, out_specs=P(("sp", "tp"), None), check_vma=False
    )
```

time: 295 us -> 83.5 us (0.28)
  the two profiles are of different devices: /device:TPU:26 before, /device:TPU:19 now
where the time goes in v1:
time: 83.5 us; the launch traced here: 83.3 us
  Pallas kernels  80.1 us (96%)
  local copies, waits for them, and re-layouts  3.2 us (4%)
    pallas_call x1, Pallas kernels, body(): pl.pallas_call(functools.partial(kernel, (S, T, td, D, hd)), out_shape=ja...  80.1 us
    unnamed x1, local copies, waits for them, and re-layouts  1.88 us

profile of v1, /device:TPU:19, one launch (start us, length us, event | category | flops | bytes accessed | tf_op | source)
XLA Modules:
  0.0 83.3 jit_solution(3756584353088475994)
XLA Ops:
  0.0 1.3 %broadcast_in_dim.2.fb_ref = f32[16,128]{1,0:T(8,128)} broadcast(f32[16]{0:T(128)} %param.14), dimensions={0} | broadcast | bytes 8256 | tf_op jit(solution)/shard_map/broadcast_in_dim | solution.py:373
  1.3 80.1 %shard_map.82 = bf16[128,2048]{1,0:T(8,128)(2,1)} custom-call(bf16[128,2048]{1,0:T(8,128)(2,1)} %x_hbm.1, bf16[2048,512]{1,0:T(8,128)(2,1)} %wq_hbm.1, bf16[2048,512]{1,0:T(8,128)(2,1)} %wk_hbm.1, bf16[2048,512]{1,0:T(8,128)(2,1)} %wv_hbm.1, bf16[2048,512]{1,0:T(8,128)(2,1)} %wg_hbm.1, bf16[16,2048]{1,0:T(8,128)(2,1)} %bitcast.1, ...), custom_call_target="tpu_custom_call" | custom-call | tf_op jit(solution)/shard_map/pallas_call | solution.py:364
  81.5 1.9 %copy.10 = bf16[128,2048]{1,0:T(8,128)(2,1)} copy(bf16[128,2048]{1,0:T(8,128)(2,1)} %shard_map.82) | data formatting | bytes 1048576

commit v2 on v1

--- a/solution.py
+++ b/solution.py
@@ -80,9 +80,21 @@
     for i, w in enumerate((wk_hbm, wv_hbm, wq_hbm, wg_hbm)):
         loads.append(pltpu.make_async_copy(w, wbuf.at[i], load_sem.at[1 + i]))
     loads.append(pltpu.make_async_copy(wo_hbm, wo, load_sem.at[5]))
-    for ld in loads:
+    for ld in loads[:4]:
         ld.start()
+    barrier = pltpu.get_barrier_semaphore()
+    me = s * T + t
+
+    def greet(i, carry):
+        to = lax.rem(me + i, S * T)
+        pl.semaphore_signal(
+            barrier, inc=1, device_id={"sp": to // T, "tp": to % T}, device_id_type=MESH
+        )
+        return carry
+
+    lax.fori_loop(1, S * T, greet, 0)
     own.wait()
+    pl.semaphore_wait(barrier, S * T - 1)
     tok_copies = []
     for dy in range(1, ny):
         dt = ((y + dy) % ny) * CORES + c
@@ -93,6 +105,10 @@
     arrived(piece(peer), tok_recv.at[peer])
 
     lane = lax.broadcasted_iota(jnp.int32, (H, gr), 1)
+    line = lax.broadcasted_iota(jnp.int32, (H, gr), 0)
+    bias = jnp.zeros((H, gr), F32)
+    for h in range(H):
+        bias = jnp.where(line == h, fb_ref[h], bias)
 
     def q_place(b):
         start = b * gr
@@ -103,8 +119,9 @@
 
     def kv_args(dy, yg, j, m):
         b = s * ny + yg
+        at = (dy * hd + j) * cph + m
+        j = (j + s) % hd
         jj = c * hd + j
-        at = (dy * hd + j) * cph + m
         dst_s = jj * cph + m
         dst_t = y * CORES + s % CORES
         base = pl.multiple_of(yg * gr, gr)
@@ -116,11 +133,13 @@
 
     def q_args(dy, yg, j):
         b = s * ny + yg
+        at = dy * hd + j
+        j = (j + s) % hd
         jj = c * hd + j
         r, pos = q_place(b)
         base = pl.multiple_of(yg * gr, gr)
         return (
-            qs_.at[j, pl.ds(base, gr)], qd.at[pl.ds(pos, gr)], q_send.at[dy * hd + j],
+            qs_.at[j, pl.ds(base, gr)], qd.at[pl.ds(pos, gr)], q_send.at[at],
             q_recv.at[pos // gr], jj * cph + r // CORES, y * CORES + r % CORES,
         )
 
@@ -152,7 +171,7 @@
             kvs[j, pl.ds(base, gr), HEAD_DIM:] = prod[:, j * HEAD_DIM : (j + 1) * HEAD_DIM].astype(BF16)
         logit = lax.dot_general(
             fw_ref[...], x, (((1,), (1,)), ((), ())), preferred_element_type=F32
-        ) + fb_ref[:, 0:1]
+        ) + bias
         logs = jnp.minimum(logit, 0.0) - jnp.log1p(jnp.exp(-jnp.abs(logit)))
         step = 1
         while step < gr:
@@ -179,6 +198,8 @@
             gs[j, pl.ds(base, gr)] = prod[:, j * HEAD_DIM : (j + 1) * HEAD_DIM]
         for e in range(CORES):
             send(*g_args(yg * CORES + e))
+        if dy == 0:
+            loads[4].start()
 
     def fwd_args(b):
         gbase = pl.multiple_of(b * gr, gr)
@@ -348,6 +369,7 @@
     vmem = pltpu.VMEM
     any_ = pl.BlockSpec(memory_space=pl.ANY)
     vm = pl.BlockSpec(memory_space=pltpu.VMEM)
+    smem = pl.BlockSpec(memory_space=pltpu.SMEM)
     scratch = [
         vmem((rows, D), BF16), vmem((4, D, width), BF16), vmem((D, D), BF16),
         vmem((hd, rows, 2 * HEAD_DIM), BF16), vmem((hd, rows, HEAD_DIM), BF16),
@@ -364,13 +386,13 @@
     return pl.pallas_call(
         functools.partial(kernel, (S, T, td, D, hd)),
         out_shape=jax.ShapeDtypeStruct((td, D), BF16),
-        in_specs=[any_, any_, any_, any_, any_, vm, vm, any_],
+        in_specs=[any_, any_, any_, any_, any_, vm, smem, any_],
         out_specs=vm,
         scratch_shapes=scratch,
         compiler_params=pltpu.CompilerParams(
-            has_side_effects=True, vmem_limit_bytes=60 * 1024 * 1024
+            has_side_effects=True, collective_id=0, vmem_limit_bytes=60 * 1024 * 1024
         ),
-    )(tokens, wq, wk, wv, wg, fw.T, jnp.broadcast_to(fb[:, None], (H, 128)), wo)
+    )(tokens, wq, wk, wv, wg, fw.T, fb, wo)
 
 
 def solution(mesh):

time: 83.5 us -> 79.7 us (0.954)
  Pallas kernels: 80.1 us -> 77.3 us
  local copies, waits for them, and re-layouts: 3.2 us -> 1.88 us
    pallas_call x1, Pallas kernels: 80.1 us -> 77.3 us  [body(): pl.pallas_call(functools.partial(kernel, (S, T, td, D, hd)), out_shape=ja...]
    broadcast_in_dim x1 -> x0, local copies, waits for them, and re-layouts: 1.32 us -> none  [body(): jnp.broadcast_to(fb[:, None], (H, 128))]
where the time goes in v2:
time: 79.7 us; the launch traced here: 79.2 us
  Pallas kernels  77.3 us (97%)
  local copies, waits for them, and re-layouts  1.88 us (2%)
    pallas_call x1, Pallas kernels, body(): pl.pallas_call(functools.partial(kernel, (S, T, td, D, hd)), out_shape=ja...  77.3 us
    unnamed x1, local copies, waits for them, and re-layouts  1.88 us

profile of v2, /device:TPU:19, one launch (start us, length us, event | category | flops | bytes accessed | tf_op | source)
XLA Modules:
  0.0 79.2 jit_solution(16169548632373285459)
XLA Ops:
  0.0 77.3 %shard_map.82 = bf16[128,2048]{1,0:T(8,128)(2,1)} custom-call(bf16[128,2048]{1,0:T(8,128)(2,1)} %x_hbm.1, bf16[2048,512]{1,0:T(8,128)(2,1)} %wq_hbm.1, bf16[2048,512]{1,0:T(8,128)(2,1)} %wk_hbm.1, bf16[2048,512]{1,0:T(8,128)(2,1)} %wv_hbm.1, bf16[2048,512]{1,0:T(8,128)(2,1)} %wg_hbm.1, bf16[16,2048]{1,0:T(8,128)(2,1)} %bitcast.1, f32[16]{0:T(128)} %fb_ref.1, ...), custom_call_target="tpu_custom_call" | custom-call | tf_op jit(solution)/shard_map/pallas_call | solution.py:386
  77.3 1.9 %copy.10 = bf16[128,2048]{1,0:T(8,128)(2,1)} copy(bf16[128,2048]{1,0:T(8,128)(2,1)} %shard_map.82) | data formatting | bytes 1048576
